TPU v7x, 32 devices: a whole 2x2x4 slice. The times are simulated.
32 devices in a mesh: ep: 8 (over z, y), tp: 4 (over x, core).
Axes of the slice: x: 2, y: 2, z: 4, core: 2. Of those that a mesh axis runs over, the one named last changes fastest.
Arguments:
- tokens: bfloat16 [64, 1024], P('ep'), may hold values from -6 to 6
- mix_gain: float32 [1024], replicated, may hold values from 0.1 to 1.9
- w_query: bfloat16 [1024, 512], P(None, 'tp'), may hold values from -0.1875 to 0.1875
- w_key: bfloat16 [1024, 512], P(None, 'tp'), may hold values from -0.1875 to 0.1875
- w_value: bfloat16 [1024, 1024], P(None, 'tp'), may hold values from -0.1875 to 0.1875
- w_ogate: bfloat16 [1024, 1024], P(None, 'tp'), may hold values from -0.1875 to 0.1875
- w_igate: bfloat16 [1024, 4], replicated, may hold values from -0.1875 to 0.1875
- w_fgate: bfloat16 [1024, 4], replicated, may hold values from -0.1875 to 0.1875
- forget_bias: float32 [4], replicated, may hold values from -1 to 3
- head_gain: float32 [1024], P('tp'), may hold values from 0.1 to 1.9
- w_out: bfloat16 [1024, 1024], P('tp'), may hold values from -0.1875 to 0.1875
- memory: float32 [64, 4, 128, 256], P('ep', 'tp'), may hold values from -0.4 to 0.4
- normalizer: float32 [64, 4, 128], P('ep', 'tp'), may hold values from -0.4 to 0.4
- running_max: float32 [64, 4], P('ep', 'tp'), may hold values from -4 to 4
- ffn_gain: float32 [1024], replicated, may hold values from 0.1 to 1.9
- route: int32 [64, 2], replicated, may hold values from 0 to 7, all different within a row; in each aligned block of 64 rows (0 to 63, 64 to 127, ...) at most 32 rows name the same one
- route_weight: float32 [64, 2], replicated, may hold values from 0.05 to 1
- w_gate: bfloat16 [8, 1024, 512], P('ep', None, 'tp'), may hold values from -0.1875 to 0.1875
- w_up: bfloat16 [8, 1024, 512], P('ep', None, 'tp'), may hold values from -0.1875 to 0.1875
- w_down: bfloat16 [8, 512, 1024], P('ep', 'tp'), may hold values from -0.25 to 0.25
Outputs:
- mixed: bfloat16 [64, 1024], P(None, 'ep')
- new_memory: float32 [64, 4, 128, 256], P('ep', 'tp')
- new_normalizer: float32 [64, 4, 128], P('ep', 'tp')
- new_max: float32 [64, 4], P('ep', 'tp')
Inputs may be any that keep to these rules, and one draw needn't show every extreme that they name: `route`: each expert is named by at most 32 routes in all, a bound that some block reaches; the two choices of a token differ.
All inputs are finite; a program needn't handle non-finite values.
Results may differ from a plain program's by a relative error of at most 0.014.
Values may be sent and summed in bfloat16 or wider, within the bound.
No kernel may reach another device: no remote copies, remote signals or barrier semaphores. Data moves between devices by JAX's collectives and lax.ppermute only.
A program may use at most 64 MiB of HBM per device.

v0:
```python
import jax
import jax.numpy as jnp
from jax import lax
from jax.sharding import PartitionSpec as P

EXPERT_CAPACITY = 32
EPS = 1e-06


def round_trip(values):
    rounded = lax.optimization_barrier(values.astype(jnp.bfloat16))
    return rounded.astype(jnp.float32)


def norm_rows(values, gain):
    floats = values.astype(jnp.float32)
    scale = lax.rsqrt(jnp.mean(floats * floats, axis=-1, keepdims=True) + EPS)
    return (floats * scale * gain).astype(jnp.bfloat16)


def slot_targets(route, expert_count, capacity):
    flat = route.reshape(-1)
    onehot = (flat[:, None] == jnp.arange(expert_count, dtype=jnp.int32)[None, :]).astype(jnp.int32)
    before = jnp.cumsum(onehot, axis=0) - onehot
    slot = jnp.sum(before * onehot, axis=1)
    return flat * capacity + slot


def shards(
    tokens,
    mix_gain,
    w_query,
    w_key,
    w_value,
    w_ogate,
    w_igate,
    w_fgate,
    forget_bias,
    head_gain,
    w_out,
    memory,
    normalizer,
    running_max,
    ffn_gain,
    route,
    route_weight,
    w_gate,
    w_up,
    w_down,
):
    width = tokens.shape[1]
    col_count = width // lax.axis_size("ep")
    qk_dim = w_query.shape[1]
    normed = norm_rows(tokens, mix_gain)
    query = round_trip(jnp.dot(normed, w_query, preferred_element_type=jnp.float32))
    scaled_key = round_trip(
        jnp.dot(normed, w_key, preferred_element_type=jnp.float32)
    ) * qk_dim ** (-0.5)
    value = round_trip(jnp.dot(normed, w_value, preferred_element_type=jnp.float32))
    ogate = round_trip(jnp.dot(normed, w_ogate, preferred_element_type=jnp.float32))
    head_pick = (jnp.arange(w_igate.shape[1], dtype=jnp.int32) == lax.axis_index("tp")).astype(
        jnp.float32
    )
    log_in = jnp.sum(
        jnp.dot(normed, w_igate, preferred_element_type=jnp.float32) * head_pick, axis=1
    )
    forget_pre = jnp.sum(
        jnp.dot(normed, w_fgate, preferred_element_type=jnp.float32) * head_pick, axis=1
    )
    log_forget = jax.nn.log_sigmoid(forget_pre + jnp.sum(forget_bias * head_pick))
    old_max = running_max[:, 0]
    new_max = jnp.maximum(log_forget + old_max, log_in)
    keep = jnp.exp(log_forget + old_max - new_max)
    admit = jnp.exp(log_in - new_max)
    state = (
        keep[:, None, None] * memory[:, 0]
        + admit[:, None, None] * scaled_key[:, :, None] * value[:, None, :]
    )
    norm_state = keep[:, None] * normalizer[:, 0] + admit[:, None] * scaled_key
    numer = jnp.einsum("tk,tkv->tv", query, state, precision=lax.Precision.HIGHEST)
    denom = jnp.sum(query * norm_state, axis=1)
    read = numer / jnp.maximum(jnp.abs(denom), jnp.exp(-new_max))[:, None]
    scale = lax.rsqrt(jnp.mean(read * read, axis=-1, keepdims=True) + EPS)
    gated = (jax.nn.sigmoid(ogate) * read * scale * head_gain).astype(jnp.bfloat16)
    local_output = lax.psum(
        jnp.dot(gated, w_out, preferred_element_type=jnp.float32).astype(jnp.bfloat16), "tp"
    ).astype(jnp.float32)
    middle_rows = (tokens.astype(jnp.float32) + local_output).astype(jnp.bfloat16)
    middle = lax.all_to_all(middle_rows, "ep", split_axis=1, concat_axis=0, tiled=True)
    expert_count = w_gate.shape[0] * lax.axis_size("ep")
    topk_count = route.shape[1]
    targets = slot_targets(route, expert_count, EXPERT_CAPACITY)
    buffer = (
        jnp.zeros((expert_count * EXPERT_CAPACITY, col_count), jnp.bfloat16)
        .at[targets]
        .set(jnp.repeat(middle, topk_count, axis=0))
    )
    buffer = buffer.reshape(expert_count, EXPERT_CAPACITY, col_count)
    rows = lax.all_to_all(buffer, "ep", split_axis=0, concat_axis=2, tiled=True)
    rows = norm_rows(rows, ffn_gain)
    gate_v = jnp.einsum("ecd,edf->ecf", rows, w_gate, preferred_element_type=jnp.float32)
    up_v = jnp.einsum("ecd,edf->ecf", rows, w_up, preferred_element_type=jnp.float32)
    activation = (jax.nn.silu(gate_v) * up_v).astype(jnp.bfloat16)
    partial_value = jnp.einsum(
        "ecf,efd->ecd", activation, w_down, preferred_element_type=jnp.float32
    )
    results = lax.psum(partial_value.astype(jnp.bfloat16), "tp")
    returned = lax.all_to_all(results, "ep", split_axis=2, concat_axis=0, tiled=True)
    picked = returned.reshape(expert_count * EXPERT_CAPACITY, col_count)[targets]
    picked = picked.reshape(route.shape[0], topk_count, col_count).astype(jnp.float32)
    weights = route_weight / jnp.sum(route_weight, axis=1, keepdims=True)
    mixed = (middle.astype(jnp.float32) + jnp.sum(picked * weights[:, :, None], axis=1)).astype(
        jnp.bfloat16
    )
    return (mixed, state[:, None], norm_state[:, None], new_max[:, None])


def solution(mesh):
    return jax.shard_map(
        shards,
        mesh=mesh,
        in_specs=(
            P("ep", None),
            P(),
            P(None, "tp"),
            P(None, "tp"),
            P(None, "tp"),
            P(None, "tp"),
            P(),
            P(),
            P(),
            P("tp"),
            P("tp", None),
            P("ep", "tp", None, None),
            P("ep", "tp", None),
            P("ep", "tp"),
            P(),
            P(),
            P(),
            P("ep", None, "tp"),
            P("ep", None, "tp"),
            P("ep", "tp", None),
        ),
        out_specs=(P(None, "ep"), P("ep", "tp", None, None), P("ep", "tp", None), P("ep", "tp")),
        check_vma=False,
    )
```

profile of v0, /device:TPU:0, one launch (start us, length us, event | category | flops | bytes accessed | tf_op | source)
XLA Modules:
  0.0 114.8 jit_solution(4171381798939121330)
XLA Ops:
  7.2 1.4 %fusion.48 = f32[]{:T(128)} fusion(f32[4]{0:T(128)} %param.28, s32[]{:T(128)S(6)} %axis_index.12), kind=kLoop, calls=%fused_computation.81 | loop fusion | flops 11 | bytes 24 | tf_op jit(solution)/shard_map/reduce_sum | solution.py:70
  8.7 0.8 fusion.28
  9.5 0.9 fusion.3
  10.4 0.9 fusion.2
  11.3 1.3 %fusion.46 = (f32[8]{0:T(128)S(1)}, f32[8]{0:T(128)S(1)}) fusion(f32[8]{0:T(128)S(1)} %fusion.3, f32[8,1]{0,1:T(1,128)} %param.33, f32[8]{0:T(128)S(1)} %fusion.2, f32[]{:T(128)} %fusion.48), kind=kLoop, calls=%fused_computation.79 | loop fusion | flops 96 | bytes 164 | tf_op jit(solution)/shard_map/exp | solution.py:73
  12.7 1.3 %exponential_bitcast_fusion = (f32[8]{0:T(128)S(1)}, f32[8,1]{0,1:T(1,128)S(1)}) fusion(f32[8]{0:T(128)S(1)} %fusion.3, f32[8,1]{0,1:T(1,128)} %param.33, f32[8]{0:T(128)S(1)} %fusion.2, f32[]{:T(128)} %fusion.48), kind=kLoop, calls=%fused_computation.104 | loop fusion | flops 96 | bytes 164 | tf_op jit(solution)/shard_map/mul | solution.py:79
  14.1 0.9 convolution_convert_fusion.5
  14.9 1.2 %convolution_convert_fusion.4 = bf16[8,128]{1,0:T(8,128)(2,1)S(1)} fusion(bf16[1024,128]{1,0:T(8,128)(2,1)} %param.23, bf16[8,1024]{1,0:T(8,128)(2,1)S(1)} %copy-done.3, f32[1024]{0:T(1024)} %param.21, f32[8]{0:T(128)S(1)} %add_rsqrt_fusion.2), kind=kOutput, calls=%fused_computation.9 | convolution fusion | flops 2130944 | bytes 284704 | tf_op jit(solution)/shard_map/dot_general | solution.py:57
  16.1 0.9 convolution_convert_fusion.2
  17.0 1.3 %convolution_convert_fusion.3 = bf16[8,256]{1,0:T(8,128)(2,1)S(1)} fusion(bf16[1024,256]{1,0:T(8,128)(2,1)} %param.25, bf16[8,1024]{1,0:T(8,128)(2,1)S(1)} %copy-done.3, f32[1024]{0:T(1024)} %param.21, f32[8]{0:T(128)S(1)} %add_rsqrt_fusion.2), kind=kOutput, calls=%fused_computation.8 | convolution fusion | flops 4229120 | bytes 548896 | tf_op jit(solution)/shard_map/dot_general | solution.py:60
  18.3 0.7 copy-done.10
  19.0 0.8 multiply_reduce_fusion.1
  19.8 0.6 fusion.5
  20.4 0.2 multiply_reduce_fusion
  20.6 0.7 copy-done.13
  21.3 0.2 convolution_convert_fusion.1
  21.5 12.7 %psum.14 = bf16[8,1024]{1,0:T(8,128)(2,1)S(1)} all-reduce(bf16[8,1024]{1,0:T(8,128)(2,1)S(1)} %convolution_convert_fusion.1), channel_id=1, replica_groups=mesh['ep'=8,'tp'=4] {'tp'}, use_global_device_ids=true, to_apply=%region_6.7 | all-reduce | flops 8192 | bytes 32768 | tf_op jit(solution)/shard_map/psum | solution.py:85
  34.2 0.6 fusion.34
  34.8 6.0 %all-to-all-start = ((bf16[8,8,128]{2,0,1:T(8,128)(2,1)}), bf16[8,8,128]{2,0,1:T(8,128)(2,1)S(1)}, u32[]{:S(2)}, u32[]{:S(2)}) async-start(bf16[8,8,128]{2,0,1:T(8,128)(2,1)} %fusion.34), calls=%async_computation | async-start | bytes 32768 | tf_op jit(solution)/shard_map/all_to_all | solution.py:89
  40.8 0.1 copy.48
  40.9 0.1 copy.47
  41.0 0.1 mul.253
  41.2 0.1 eq.27
  41.4 0.2 reduce_window_sum.11
  41.6 0.2 select_reduce_fusion
  41.8 5.6 %all-to-all-done = bf16[8,8,128]{2,0,1:T(8,128)(2,1)S(1)} async-done(((bf16[8,8,128]{2,0,1:T(8,128)(2,1)}), bf16[8,8,128]{2,0,1:T(8,128)(2,1)S(1)}, u32[]{:S(2)}, u32[]{:S(2)}) %all-to-all-start) | async-done | bytes 16416 | tf_op jit(solution)/shard_map/all_to_all | solution.py:89
  47.4 0.9 scatter_custom_fusion
  48.3 9.3 %all_to_all.43 = bf16[8,32,128]{2,1,0:T(8,128)(2,1)S(1)} all-to-all(bf16[8,32,128]{2,1,0:T(8,128)(2,1)S(1)} %bitcast.126), channel_id=1, replica_groups=mesh['ep'=8,'tp'=4] {'ep'}, dimensions={0} | all-to-all | bytes 131072 | tf_op jit(solution)/shard_map/all_to_all | solution.py:99
  57.6 0.1 fusion.16
  57.7 0.6 copy-done.7
  58.4 0.2 fusion.14
  58.6 0.6 copy-done.6
  59.2 0.1 copy-done.5
  59.3 0.9 fusion
  60.3 1.2 %multiply_add_fusion = f32[8,1,128,256]{3,2,1,0:T(8,128)} fusion(f32[8,1,128,256]{3,2,1,0:T(8,128)S(1)} %copy-done.1, f32[8,256]{1,0:T(8,128)S(1)} %convert_element_type.117, f32[8,128]{1,0:T(8,128)S(1)} %get-tuple-element.30, f32[8]{0:T(128)S(1)} %get-tuple-element.24), kind=kLoop, calls=%fused_computation.18 | loop fusion | flops 786432 | bytes 2109472 | tf_op jit(solution)/shard_map/add | solution.py:76
  61.5 27.0 %all-reduce.2.cloned.1.call-done = bf16[1,32,1024]{2,1,0:T(8,128)(2,1)} async-done(((bf16[1,32,1024]{2,1,0:T(8,128)(2,1)}), bf16[1,32,1024]{2,1,0:T(8,128)(2,1)}) %all-reduce.2.cloned.1.call-update) | async-done | bytes 65552 | tf_op jit(solution)/shard_map/psum | solution.py:107
  88.5 1.1 copy.50
  89.6 0.5 broadcast.215
  90.1 2.3 %reduce.3 = bf16[1024,32]{1,0:T(8,128)(2,1)S(1)} reduce(bf16[1024,1,32]{2,1,0:T(2,128)(2,1)S(1)} %bitcast.121, bf16[]{:T(256)} %broadcast.215), dimensions={1}, to_apply=%bitcast.105.reduce_sub_computation | reduce | bytes 131074
  92.4 0.9 reshape.303
  93.3 5.5 %all-to-all-start.2 = ((bf16[8,2,2048]{2,1,0:T(2,128)(2,1)}), bf16[8,2,2048]{2,1,0:T(2,128)(2,1)S(1)}, u32[]{:S(2)}, u32[]{:S(2)}) async-start(bf16[8,2,2048]{2,1,0:T(2,128)(2,1)} %reshape.303), calls=%async_computation.2 | async-start | bytes 131072 | tf_op jit(solution)/shard_map/all_to_all | solution.py:108
  98.8 0.1 copy.53
  99.0 6.8 %all-to-all-done.2 = bf16[8,2,2048]{2,1,0:T(2,128)(2,1)S(1)} async-done(((bf16[8,2,2048]{2,1,0:T(2,128)(2,1)}), bf16[8,2,2048]{2,1,0:T(2,128)(2,1)S(1)}, u32[]{:S(2)}, u32[]{:S(2)}) %all-to-all-start.2) | async-done | bytes 65568 | tf_op jit(solution)/shard_map/all_to_all | solution.py:108
  105.7 0.3 reshape.304
  106.1 0.3 copy.51
  106.4 0.7 gather_fusion
  107.2 0.1 fusion.23
  107.3 0.6 add_convert_fusion
  (45 shorter events, 0.5 us)
Async XLA Ops:
  7.2 13.5 %copy-start = (bf16[256,1024]{1,0:T(8,128)(2,1)S(1)}, bf16[256,1024]{1,0:T(8,128)(2,1)}, u32[]{:S(2)}) copy-start(bf16[256,1024]{1,0:T(8,128)(2,1)} %param.30) | copy-start | bytes 1572868
  7.2 2.3 %copy-start.3 = (bf16[8,1024]{1,0:T(8,128)(2,1)S(1)}, bf16[8,1024]{1,0:T(8,128)(2,1)}, u32[]{:S(2)}) copy-start(bf16[8,1024]{1,0:T(8,128)(2,1)} %param.20) | copy-start | bytes 49156
  7.2 6.8 %copy-start.12 = (bf16[1024,128]{1,0:T(8,128)(2,1)S(1)}, bf16[1024,128]{1,0:T(8,128)(2,1)}, u32[]{:S(2)}) copy-start(bf16[1024,128]{1,0:T(8,128)(2,1)} %param.22) | copy-start | bytes 786436
  7.2 8.9 %copy-start.2 = (bf16[1024,256]{1,0:T(8,128)(2,1)S(1)}, bf16[1024,256]{1,0:T(8,128)(2,1)}, u32[]{:S(2)}) copy-start(bf16[1024,256]{1,0:T(8,128)(2,1)} %param.24) | copy-start | bytes 1572868
  7.2 12.6 %copy-start.1 = (f32[8,1,128,256]{3,2,1,0:T(8,128)S(1)}, f32[8,1,128,256]{3,2,1,0:T(8,128)}, u32[]{:S(2)}) copy-start(f32[8,1,128,256]{3,2,1,0:T(8,128)} %param.31) | copy-start | bytes 3145732
  14.0 5.8 %copy-start.11 = (f32[8,1]{0,1:T(1,128)}, f32[8,1]{0,1:T(1,128)S(1)}, u32[]{:S(2)}) copy-start(f32[8,1]{0,1:T(1,128)S(1)} %get-tuple-element.29) | copy-start | bytes 100
  18.3 0.7 copy-start.10
  20.6 0.7 copy-start.13
  34.8 6.0 %copy-start.8 = (s32[64,2]{0,1:T(2,128)S(1)}, s32[64,2]{0,1:T(2,128)}, u32[]{:S(2)}) copy-start(s32[64,2]{0,1:T(2,128)} %param.35) | copy-start | bytes 1540
  34.8 12.5 %all-to-all-start = ((bf16[8,8,128]{2,0,1:T(8,128)(2,1)}), bf16[8,8,128]{2,0,1:T(8,128)(2,1)S(1)}, u32[]{:S(2)}, u32[]{:S(2)}) async-start(bf16[8,8,128]{2,0,1:T(8,128)(2,1)} %fusion.34), calls=%async_computation | async-start | bytes 32768 | tf_op jit(solution)/shard_map/all_to_all | solution.py:89
  40.8 47.7 %all-reduce.2.cloned.1.call-start = ((), (), s32[]{:S(2)}) async-start(), calls=%async_computation.3 | async-start | bytes 131072 | tf_op jit(solution)/shard_map/psum | solution.py:107
  47.4 11.0 %copy-start.4 = (bf16[1,1024,128]{2,1,0:T(8,128)(2,1)S(1)}, bf16[1,1024,128]{2,1,0:T(8,128)(2,1)}, u32[]{:S(2)}) copy-start(bf16[1,1024,128]{2,1,0:T(8,128)(2,1)} %param.37) | copy-start | bytes 786436
  57.6 0.7 copy-start.7
  58.3 0.9 copy-start.6
  58.4 1.0 copy-start.5
  60.3 1.2 %copy-start.9 = (f32[64,2]{0,1:T(2,128)S(1)}, f32[64,2]{0,1:T(2,128)}, u32[]{:S(2)}) copy-start(f32[64,2]{0,1:T(2,128)} %param.36) | copy-start | bytes 1540
  93.3 12.4 %all-to-all-start.2 = ((bf16[8,2,2048]{2,1,0:T(2,128)(2,1)}), bf16[8,2,2048]{2,1,0:T(2,128)(2,1)S(1)}, u32[]{:S(2)}, u32[]{:S(2)}) async-start(bf16[8,2,2048]{2,1,0:T(2,128)(2,1)} %reshape.303), calls=%async_computation.2 | async-start | bytes 131072 | tf_op jit(solution)/shard_map/all_to_all | solution.py:108
Sparse Core Ops, SparseCore 0:
  60.4 28.0 all-reduce.1
where the time goes:
time: 116 us; the launch traced here: 115 us
  waiting for transfers between devices  39.4 us (34%)
  blocking collectives  22 us (19%)
  between operations  14.3 us (12%)
  starting transfers between devices  11.5 us (10%)
  other arithmetic  11.4 us (10%)
  local copies, waits for them, and re-layouts  8.14 us (7%)
  matrix products  7.98 us (7%)
    psum x1, waiting for transfers between devices, shards(): results = lax.psum(partial_value.astype(jnp.bfloat16), 'tp')  27 us
    psum x1, blocking collectives, shards(): lax.psum(jnp.dot(gated, w_out, preferred_element_type=jnp.float32).astype...  12.7 us
    all_to_all x1, blocking collectives, shards(): rows = lax.all_to_all(buffer, 'ep', split_axis=0, concat_axis=2, tiled=True)  9.29 us
    all_to_all x1, waiting for transfers between devices, shards(): lax.all_to_all(results, 'ep', split_axis=2, concat_axis=0, tiled=True)  6.79 us
    all_to_all x1, starting transfers between devices, shards(): lax.all_to_all(middle_rows, 'ep', split_axis=1, concat_axis=0, tiled=True)  5.97 us
    all_to_all x1, waiting for transfers between devices, shards(): lax.all_to_all(middle_rows, 'ep', split_axis=1, concat_axis=0, tiled=True)  5.58 us
    all_to_all x1, starting transfers between devices, shards(): lax.all_to_all(results, 'ep', split_axis=2, concat_axis=0, tiled=True)  5.52 us
    unnamed x33, local copies, waits for them, and re-layouts  4.59 us
  transfers between devices with their start and end apart: 3, of which 3 were waited for; matrix products, arithmetic and copies ran while one was open for 2% of the time, Pallas kernels for 0%

commit v1 on v0

--- a/solution.py
+++ b/solution.py
@@ -104,7 +104,7 @@
     partial_value = jnp.einsum(
         "ecf,efd->ecd", activation, w_down, preferred_element_type=jnp.float32
     )
-    results = lax.psum(partial_value.astype(jnp.bfloat16), "tp")
+    results = jnp.sum(lax.all_gather(partial_value.astype(jnp.bfloat16), "tp"), axis=0)
     returned = lax.all_to_all(results, "ep", split_axis=2, concat_axis=0, tiled=True)
     picked = returned.reshape(expert_count * EXPERT_CAPACITY, col_count)[targets]
     picked = picked.reshape(route.shape[0], topk_count, col_count).astype(jnp.float32)

time: 116 us -> 77.2 us (0.67)
  waiting for transfers between devices: 39.4 us -> 17.9 us
  between operations: 14.3 us -> 0.98 us
  blocking collectives: 22 us -> 18.5 us
  starting transfers between devices: 11.5 us -> 12.7 us
    psum x1 -> x0, waiting for transfers between devices: 27 us -> none  [shards(): results = lax.psum(partial_value.astype(jnp.bfloat16), 'tp')]
    all_to_all x1 -> x0, blocking collectives: 9.29 us -> none  [shards(): rows = lax.all_to_all(buffer, 'ep', split_axis=0, concat_axis=2, tiled=True)]
    all_gather x0 -> x1, blocking collectives: none -> 5.78 us  [shards(): lax.all_gather(partial_value.astype(jnp.bfloat16), 'tp')]
    all_to_all x0 -> x1, waiting for transfers between devices: none -> 5.59 us  [shards(): rows = lax.all_to_all(buffer, 'ep', split_axis=0, concat_axis=2, tiled=True)]
    all_to_all x0 -> x1, starting transfers between devices: none -> 3.35 us  [shards(): rows = lax.all_to_all(buffer, 'ep', split_axis=0, concat_axis=2, tiled=True)]
    all_to_all x1, starting transfers between devices: 5.52 us -> 3.35 us  [shards(): lax.all_to_all(results, 'ep', split_axis=2, concat_axis=0, tiled=True)]
  transfers between devices with their start and end apart: 3 -> 3, of which waited for: 3 -> 3; matrix products, arithmetic and copies ran while one was open for 2% -> 3% of each run, Pallas kernels for 0% -> 0%
where the time goes in v1:
time: 77.2 us; the launch traced here: 76.3 us
  blocking collectives  18.5 us (24%)
  waiting for transfers between devices  17.9 us (23%)
  starting transfers between devices  12.7 us (16%)
  other arithmetic  11.5 us (15%)
  local copies, waits for them, and re-layouts  7.39 us (10%)
  matrix products  7.34 us (10%)
  between operations  0.98 us (1%)
    psum x1, blocking collectives, shards(): lax.psum(jnp.dot(gated, w_out, preferred_element_type=jnp.float32).astype...  12.7 us
    all_to_all x1, waiting for transfers between devices, shards(): lax.all_to_all(results, 'ep', split_axis=2, concat_axis=0, tiled=True)  6.73 us
    all_to_all x1, starting transfers between devices, shards(): lax.all_to_all(middle_rows, 'ep', split_axis=1, concat_axis=0, tiled=True)  5.97 us
    all_gather x1, blocking collectives, shards(): lax.all_gather(partial_value.astype(jnp.bfloat16), 'tp')  5.78 us
    all_to_all x1, waiting for transfers between devices, shards(): lax.all_to_all(middle_rows, 'ep', split_axis=1, concat_axis=0, tiled=True)  5.63 us
    all_to_all x1, waiting for transfers between devices, shards(): rows = lax.all_to_all(buffer, 'ep', split_axis=0, concat_axis=2, tiled=True)  5.59 us
    unnamed x33, local copies, waits for them, and re-layouts  4.02 us
    all_to_all x1, starting transfers between devices, shards(): rows = lax.all_to_all(buffer, 'ep', split_axis=0, concat_axis=2, tiled=True)  3.35 us
  transfers between devices with their start and end apart: 3, of which 3 were waited for; matrix products, arithmetic and copies ran while one was open for 3% of the time, Pallas kernels for 0%

profile of v1, /device:TPU:0, one launch (start us, length us, event | category | flops | bytes accessed | tf_op | source)
XLA Modules:
  0.0 76.3 jit_solution(18295127185329042904)
XLA Ops:
  0.7 1.4 %fusion.47 = f32[]{:T(128)} fusion(f32[4]{0:T(128)} %param.28, s32[]{:T(128)S(6)} %axis_index.12), kind=kLoop, calls=%fused_computation.80 | loop fusion | flops 11 | bytes 24 | tf_op jit(solution)/shard_map/reduce_sum | solution.py:70
  2.1 0.8 %fusion.27 = f32[8]{0:T(128)S(1)} fusion(bf16[8,1024]{1,0:T(8,128)(2,1)} %param.20), kind=kLoop, calls=%fused_computation.45 | loop fusion | flops 24568 | bytes 16416 | tf_op jit(solution)/shard_map/reduce_sum | solution.py:17
  3.0 0.9 %fusion.2 = f32[8]{0:T(128)S(1)} fusion(bf16[1024,4]{0,1:T(4,128)(2,1)} %param.26, f32[4]{0:T(128)S(1)} %compare_convert_fusion, bf16[8,1024]{1,0:T(8,128)(2,1)S(1)} %copy-done.3, f32[1024]{0:T(1024)} %param.21, f32[8]{0:T(128)S(1)} %add_rsqrt_fusion.2), kind=kOutput, calls=%fused_computation.13 | convolution fusion | flops 98360 | bytes 28752 | tf_op jit(solution)/shard_map/dot_general | solution.py:65
  3.9 0.9 %fusion.1 = f32[8]{0:T(128)S(1)} fusion(bf16[1024,4]{0,1:T(4,128)(2,1)} %param.27, f32[4]{0:T(128)S(1)} %compare_convert_fusion, bf16[8,1024]{1,0:T(8,128)(2,1)S(1)} %copy-done.3, f32[1024]{0:T(1024)} %param.21, f32[8]{0:T(128)S(1)} %add_rsqrt_fusion.2), kind=kOutput, calls=%fused_computation.12 | convolution fusion | flops 98360 | bytes 28752 | tf_op jit(solution)/shard_map/dot_general | solution.py:68
  4.8 1.3 %fusion.45 = (f32[8]{0:T(128)S(1)}, f32[8]{0:T(128)S(1)}) fusion(f32[8]{0:T(128)S(1)} %fusion.2, f32[8,1]{0,1:T(1,128)} %param.33, f32[8]{0:T(128)S(1)} %fusion.1, f32[]{:T(128)} %fusion.47), kind=kLoop, calls=%fused_computation.78 | loop fusion | flops 96 | bytes 164 | tf_op jit(solution)/shard_map/exp | solution.py:73
  6.1 1.3 %exponential_bitcast_fusion = (f32[8]{0:T(128)S(1)}, f32[8,1]{0,1:T(1,128)S(1)}) fusion(f32[8]{0:T(128)S(1)} %fusion.2, f32[8,1]{0,1:T(1,128)} %param.33, f32[8]{0:T(128)S(1)} %fusion.1, f32[]{:T(128)} %fusion.47), kind=kLoop, calls=%fused_computation.103 | loop fusion | flops 96 | bytes 164 | tf_op jit(solution)/shard_map/mul | solution.py:79
  7.5 0.9 %convolution_convert_fusion.5 = bf16[8,128]{1,0:T(8,128)(2,1)S(1)} fusion(bf16[1024,128]{1,0:T(8,128)(2,1)S(1)} %copy-done.12, bf16[8,1024]{1,0:T(8,128)(2,1)S(1)} %copy-done.3, f32[1024]{0:T(1024)} %param.21, f32[8]{0:T(128)S(1)} %add_rsqrt_fusion.2), kind=kOutput, calls=%fused_computation.9 | convolution fusion | flops 2130944 | bytes 284704 | tf_op jit(solution)/shard_map/dot_general | solution.py:55
  8.4 1.2 %convolution_convert_fusion.4 = bf16[8,128]{1,0:T(8,128)(2,1)S(1)} fusion(bf16[1024,128]{1,0:T(8,128)(2,1)} %param.23, bf16[8,1024]{1,0:T(8,128)(2,1)S(1)} %copy-done.3, f32[1024]{0:T(1024)} %param.21, f32[8]{0:T(128)S(1)} %add_rsqrt_fusion.2), kind=kOutput, calls=%fused_computation.8 | convolution fusion | flops 2130944 | bytes 284704 | tf_op jit(solution)/shard_map/dot_general | solution.py:57
  9.6 0.9 %convolution_convert_fusion.2 = bf16[8,256]{1,0:T(8,128)(2,1)S(1)} fusion(bf16[1024,256]{1,0:T(8,128)(2,1)S(1)} %copy-done.2, bf16[8,1024]{1,0:T(8,128)(2,1)S(1)} %copy-done.3, f32[1024]{0:T(1024)} %param.21, f32[8]{0:T(128)S(1)} %add_rsqrt_fusion.2), kind=kOutput, calls=%fused_computation.6 | convolution fusion | flops 4229120 | bytes 548896 | tf_op jit(solution)/shard_map/dot_general | solution.py:59
  10.5 1.3 %convolution_convert_fusion.3 = bf16[8,256]{1,0:T(8,128)(2,1)S(1)} fusion(bf16[1024,256]{1,0:T(8,128)(2,1)} %param.25, bf16[8,1024]{1,0:T(8,128)(2,1)S(1)} %copy-done.3, f32[1024]{0:T(1024)} %param.21, f32[8]{0:T(128)S(1)} %add_rsqrt_fusion.2), kind=kOutput, calls=%fused_computation.7 | convolution fusion | flops 4229120 | bytes 548896 | tf_op jit(solution)/shard_map/dot_general | solution.py:60
  11.8 0.7 copy-done.10
  12.5 0.8 %multiply_reduce_fusion.1 = (f32[8]{0:T(128)S(1)}, f32[8,128]{1,0:T(8,128)}, f32[8,128]{1,0:T(8,128)S(1)}) fusion(bf16[8,128]{1,0:T(8,128)(2,1)S(1)} %convolution_convert_fusion.5, f32[8]{0:T(128)S(1)} %fusion.60, bf16[8,128]{1,0:T(8,128)(2,1)S(1)} %convolution_convert_fusion.4, f32[8,128]{1,0:T(8,128)S(1)} %bitcast.134, f32[8]{0:T(128)S(1)} %get-tuple-element.28, ...), kind=kLoop, calls=%fused_computation.69 | loop fusion | flops 8184 | bytes 16512 | tf_op jit(solution)/shard_map/reduce_sum | solution.py:81
  13.3 0.6 fusion.4
  13.9 0.2 multiply_reduce_fusion
  14.1 0.7 copy-done.13
  14.8 0.2 convolution_convert_fusion.1
  15.0 12.7 %psum.7 = bf16[8,1024]{1,0:T(8,128)(2,1)S(1)} all-reduce(bf16[8,1024]{1,0:T(8,128)(2,1)S(1)} %convolution_convert_fusion.1), channel_id=1, replica_groups=mesh['ep'=8,'tp'=4] {'tp'}, use_global_device_ids=true, to_apply=%region_6.7 | all-reduce | flops 8192 | bytes 32768 | tf_op jit(solution)/shard_map/psum | solution.py:85
  27.7 0.6 fusion.33
  28.3 6.0 %all-to-all-start = ((bf16[8,8,128]{2,0,1:T(8,128)(2,1)}), bf16[8,8,128]{2,0,1:T(8,128)(2,1)S(1)}, u32[]{:S(2)}, u32[]{:S(2)}) async-start(bf16[8,8,128]{2,0,1:T(8,128)(2,1)} %fusion.33), calls=%async_computation | async-start | bytes 32768 | tf_op jit(solution)/shard_map/all_to_all | solution.py:89
  34.3 0.1 copy.47
  34.4 0.1 copy.46
  34.4 0.1 mul.253
  34.6 0.1 eq.27
  34.7 0.1 fusion.23
  34.8 0.2 reduce_window_sum.11
  35.0 0.2 select_reduce_fusion
  35.2 5.6 %all-to-all-done = bf16[8,8,128]{2,0,1:T(8,128)(2,1)S(1)} async-done(((bf16[8,8,128]{2,0,1:T(8,128)(2,1)}), bf16[8,8,128]{2,0,1:T(8,128)(2,1)S(1)}, u32[]{:S(2)}, u32[]{:S(2)}) %all-to-all-start) | async-done | bytes 16416 | tf_op jit(solution)/shard_map/all_to_all | solution.py:89
  40.8 1.5 %scatter_custom_fusion = bf16[256,128]{1,0:T(8,128)(2,1)} fusion(s32[128]{0:T(128)S(1)} %fusion.52, bf16[128,128]{1,0:T(8,128)(2,1)S(1)} %bitcast.131, bf16[]{:T(256)} %constant.37.clone.1), kind=kCustom, calls=%fused_computation.50 | custom fusion | bytes 65538 | tf_op jit(solution)/shard_map/scatter | solution.py:96
  42.3 3.3 %all-to-all-start.1 = ((bf16[8,32,128]{2,1,0:T(8,128)(2,1)}), bf16[8,32,128]{2,1,0:T(8,128)(2,1)S(1)}, u32[]{:S(2)}, u32[]{:S(2)}) async-start(bf16[8,32,128]{2,1,0:T(8,128)(2,1)} %bitcast.18), calls=%async_computation.1 | async-start | bytes 131072 | tf_op jit(solution)/shard_map/all_to_all | solution.py:99
  45.7 1.2 %multiply_add_fusion = f32[8,1,128,256]{3,2,1,0:T(8,128)} fusion(f32[8,1,128,256]{3,2,1,0:T(8,128)S(1)} %copy-done.1, f32[8,256]{1,0:T(8,128)S(1)} %convert_element_type.117, f32[8,128]{1,0:T(8,128)S(1)} %get-tuple-element.30, f32[8]{0:T(128)S(1)} %get-tuple-element.24), kind=kLoop, calls=%fused_computation.17 | loop fusion | flops 786432 | bytes 2109472 | tf_op jit(solution)/shard_map/add | solution.py:76
  46.9 5.6 %all-to-all-done.1 = bf16[8,32,128]{2,1,0:T(8,128)(2,1)S(1)} async-done(((bf16[8,32,128]{2,1,0:T(8,128)(2,1)}), bf16[8,32,128]{2,1,0:T(8,128)(2,1)S(1)}, u32[]{:S(2)}, u32[]{:S(2)}) %all-to-all-start.1) | async-done | bytes 65568 | tf_op jit(solution)/shard_map/all_to_all | solution.py:99
  52.5 0.1 fusion.15
  52.8 0.2 fusion.13
  53.0 0.7 copy-done.5
  53.7 0.3 convolution_convert_fusion
  54.0 5.8 %all-gather = bf16[128,1024]{1,0:T(8,128)(2,1)S(1)} all-gather(bf16[32,1024]{1,0:T(8,128)(2,1)S(1)} %convolution_convert_fusion), channel_id=2, replica_groups=mesh['ep'=8,'tp'=4] {'tp'}, dimensions={0}, use_global_device_ids=true | all-gather | bytes 327680 | tf_op jit(solution)/shard_map/all_gather | solution.py:107
  59.8 0.4 copy.49
  60.2 0.5 broadcast.215
  60.7 2.3 %reduce.6 = bf16[1024,32]{1,0:T(8,128)(2,1)S(1)} reduce(bf16[1024,1,32]{2,1,0:T(2,128)(2,1)S(1)} %bitcast.121, bf16[]{:T(256)} %broadcast.215), dimensions={1}, to_apply=%bitcast.105.reduce_sub_computation | reduce | bytes 131074
  63.0 0.9 %reshape.307 = bf16[8,2,2048]{2,1,0:T(2,128)(2,1)} reshape(bf16[1024,32]{1,0:T(8,128)(2,1)S(1)} %reduce.6) | data formatting | bytes 131072
  63.9 3.3 %all-to-all-start.2 = ((bf16[8,2,2048]{2,1,0:T(2,128)(2,1)}), bf16[8,2,2048]{2,1,0:T(2,128)(2,1)S(1)}, u32[]{:S(2)}, u32[]{:S(2)}) async-start(bf16[8,2,2048]{2,1,0:T(2,128)(2,1)} %reshape.307), calls=%async_computation.2 | async-start | bytes 131072 | tf_op jit(solution)/shard_map/all_to_all | solution.py:108
  67.3 0.1 copy.52
  67.4 6.7 %all-to-all-done.2 = bf16[8,2,2048]{2,1,0:T(2,128)(2,1)S(1)} async-done(((bf16[8,2,2048]{2,1,0:T(2,128)(2,1)}), bf16[8,2,2048]{2,1,0:T(2,128)(2,1)S(1)}, u32[]{:S(2)}, u32[]{:S(2)}) %all-to-all-start.2) | async-done | bytes 65568 | tf_op jit(solution)/shard_map/all_to_all | solution.py:108
  74.1 0.3 reshape.308
  74.4 0.3 copy.50
  74.8 0.7 gather_fusion
  75.5 0.1 fusion.22
  75.7 0.6 add_convert_fusion
  (45 shorter events, 0.4 us)
Async XLA Ops:
  0.6 13.5 %copy-start = (bf16[256,1024]{1,0:T(8,128)(2,1)S(1)}, bf16[256,1024]{1,0:T(8,128)(2,1)}, u32[]{:S(2)}) copy-start(bf16[256,1024]{1,0:T(8,128)(2,1)} %param.30) | copy-start | bytes 1572868
  0.6 2.3 %copy-start.3 = (bf16[8,1024]{1,0:T(8,128)(2,1)S(1)}, bf16[8,1024]{1,0:T(8,128)(2,1)}, u32[]{:S(2)}) copy-start(bf16[8,1024]{1,0:T(8,128)(2,1)} %param.20) | copy-start | bytes 49156
  0.7 6.8 %copy-start.12 = (bf16[1024,128]{1,0:T(8,128)(2,1)S(1)}, bf16[1024,128]{1,0:T(8,128)(2,1)}, u32[]{:S(2)}) copy-start(bf16[1024,128]{1,0:T(8,128)(2,1)} %param.22) | copy-start | bytes 786436
  0.7 8.9 %copy-start.2 = (bf16[1024,256]{1,0:T(8,128)(2,1)S(1)}, bf16[1024,256]{1,0:T(8,128)(2,1)}, u32[]{:S(2)}) copy-start(bf16[1024,256]{1,0:T(8,128)(2,1)} %param.24) | copy-start | bytes 1572868
  0.7 12.6 %copy-start.1 = (f32[8,1,128,256]{3,2,1,0:T(8,128)S(1)}, f32[8,1,128,256]{3,2,1,0:T(8,128)}, u32[]{:S(2)}) copy-start(f32[8,1,128,256]{3,2,1,0:T(8,128)} %param.31) | copy-start | bytes 3145732
  7.5 5.8 %copy-start.11 = (f32[8,1]{0,1:T(1,128)}, f32[8,1]{0,1:T(1,128)S(1)}, u32[]{:S(2)}) copy-start(f32[8,1]{0,1:T(1,128)S(1)} %get-tuple-element.29) | copy-start | bytes 100
  11.8 0.7 copy-start.10
  14.1 0.7 copy-start.13
  28.3 6.0 %copy-start.8 = (s32[64,2]{0,1:T(2,128)S(1)}, s32[64,2]{0,1:T(2,128)}, u32[]{:S(2)}) copy-start(s32[64,2]{0,1:T(2,128)} %param.35) | copy-start | bytes 1540
  28.3 12.5 %all-to-all-start = ((bf16[8,8,128]{2,0,1:T(8,128)(2,1)}), bf16[8,8,128]{2,0,1:T(8,128)(2,1)S(1)}, u32[]{:S(2)}, u32[]{:S(2)}) async-start(bf16[8,8,128]{2,0,1:T(8,128)(2,1)} %fusion.33), calls=%async_computation | async-start | bytes 32768 | tf_op jit(solution)/shard_map/all_to_all | solution.py:89
  42.3 10.2 %all-to-all-start.1 = ((bf16[8,32,128]{2,1,0:T(8,128)(2,1)}), bf16[8,32,128]{2,1,0:T(8,128)(2,1)S(1)}, u32[]{:S(2)}, u32[]{:S(2)}) async-start(bf16[8,32,128]{2,1,0:T(8,128)(2,1)} %bitcast.18), calls=%async_computation.1 | async-start | bytes 131072 | tf_op jit(solution)/shard_map/all_to_all | solution.py:99
  45.7 1.2 %copy-start.9 = (f32[64,2]{0,1:T(2,128)S(1)}, f32[64,2]{0,1:T(2,128)}, u32[]{:S(2)}) copy-start(f32[64,2]{0,1:T(2,128)} %param.36) | copy-start | bytes 1540
  45.7 7.0 %copy-start.7 = (f32[1024]{0:T(1024)S(1)}, f32[1024]{0:T(1024)}, u32[]{:S(2)}) copy-start(f32[1024]{0:T(1024)} %param.34) | copy-start | bytes 12292
  45.7 7.3 %copy-start.6 = (bf16[1,1024,128]{2,1,0:T(8,128)(2,1)S(1)}, bf16[1,1024,128]{2,1,0:T(8,128)(2,1)}, u32[]{:S(2)}) copy-start(bf16[1,1024,128]{2,1,0:T(8,128)(2,1)} %param.38) | copy-start | bytes 786436
  46.9 5.9 %copy-start.4 = (bf16[1,1024,128]{2,1,0:T(8,128)(2,1)S(1)}, bf16[1,1024,128]{2,1,0:T(8,128)(2,1)}, u32[]{:S(2)}) copy-start(bf16[1,1024,128]{2,1,0:T(8,128)(2,1)} %param.37) | copy-start | bytes 786436
  52.7 1.0 %copy-start.5 = (bf16[1,128,1024]{2,1,0:T(8,128)(2,1)S(1)}, bf16[1,128,1024]{2,1,0:T(8,128)(2,1)}, u32[]{:S(2)}) copy-start(bf16[1,128,1024]{2,1,0:T(8,128)(2,1)} %param.39) | copy-start | bytes 786436
  63.9 10.2 %all-to-all-start.2 = ((bf16[8,2,2048]{2,1,0:T(2,128)(2,1)}), bf16[8,2,2048]{2,1,0:T(2,128)(2,1)S(1)}, u32[]{:S(2)}, u32[]{:S(2)}) async-start(bf16[8,2,2048]{2,1,0:T(2,128)(2,1)} %reshape.307), calls=%async_computation.2 | async-start | bytes 131072 | tf_op jit(solution)/shard_map/all_to_all | solution.py:108
